TPU v7x, 32 devices: a whole 2x2x4 slice. The times are simulated.
32 devices in a mesh: ep: 4 (over y, x), tp: 8 (over z, core).
Axes of the slice: x: 2, y: 2, z: 4, core: 2. Of those that a mesh axis runs over, the one named last changes fastest.
Arguments:
- pool_input: bfloat16 [4096, 1024], P('ep', 'tp'), may hold values from -6 to 6
- pool_gain: float32 [1024], P('tp'), may hold values from 0.1 to 1.9
- mix_weight: bfloat16 [1024, 2048], P('tp'), may hold values from -0.1875 to 0.1875
- moe_input: bfloat16 [8192, 2048], P(('ep', 'tp')), may hold values from -6 to 6
- moe_gain: float32 [2048], replicated, may hold values from 0.1 to 1.9
- expert_ids: int32 [8192, 2], P(('ep', 'tp')), may hold values from 0 to 15, as said below
- route_weight: float32 [8192, 2], P(('ep', 'tp')), may hold values from 0.2 to 1
- gate_weight: bfloat16 [16, 2048, 1024], P('ep', None, 'tp'), may hold values from -0.125 to 0.125
- up_weight: bfloat16 [16, 2048, 1024], P('ep', None, 'tp'), may hold values from -0.125 to 0.125
- down_weight: bfloat16 [16, 2048, 1024], P('ep', None, 'tp'), may hold values from -0.1875 to 0.1875
Outputs:
- mixed_out: bfloat16 [4096, 2048], P(('ep', 'tp'))
- moe_out: bfloat16 [8192, 2048], P(('ep', 'tp'))
Inputs may be any that keep to these rules, and one draw needn't show every extreme that they name: `expert_ids`: each row names 2 different experts of one group of 4 consecutive experts. In each aligned block of 256 rows (the rows of one device) no expert is named by more than 48 rows, and some expert is named by exactly 48 rows.
All inputs are finite; a program needn't handle non-finite values.
Results may differ from a plain program's by a relative error of at most 0.012.
Values may be sent and summed in bfloat16 or wider, within the bound.
A program may use at most 128 MiB of HBM per device.

v0:
```python
import jax
import jax.numpy as jnp
from jax import lax
from jax.sharding import PartitionSpec as P

GROUP_CH = 256
EXPERTS = 16
GROUP_EXP = 4
TOP = 2
CAP = 48
eps_norm = 1e-06


def from_behind(shard, axis, by):
    peers = lax.axis_size(axis)
    pairs = [(i, i + by) for i in range(peers) if 0 <= i + by < peers]
    return lax.ppermute(shard, axis, pairs)


def window_sums(extended, row_count):
    level_sum = extended
    stride = 1
    outputs = []
    for doubling in range(4):
        level_sum = level_sum[stride:] + level_sum[:-stride]
        stride = stride * 2
        outputs.append(level_sum[level_sum.shape[0] - row_count :])
    return outputs


def pool_mixer(pool_input, pool_gain):
    row_count, channels = pool_input.shape
    carried = from_behind(pool_input[row_count - 15 :], "ep", 1)
    extended = jnp.concatenate([carried, pool_input], axis=0).astype(jnp.float32)
    window_list = window_sums(extended, row_count)
    channel_ids = lax.axis_index("tp") * channels + lax.iota(jnp.int32, channels)
    group_ids = channel_ids // GROUP_CH
    position = lax.axis_index("ep") * row_count + lax.iota(jnp.int32, row_count)
    summed = jnp.zeros((row_count, channels), jnp.float32)
    widths = jnp.zeros((channels,), jnp.int32)
    for index_group in range(4):
        inside = group_ids == index_group
        summed = jnp.where(inside[None, :], window_list[index_group], summed)
        widths = jnp.where(inside, 2 ** (index_group + 1), widths)
    counted = jnp.minimum(position[:, None] + 1, widths[None, :]).astype(jnp.float32)
    values = extended[15:]
    return ((summed / counted - values) * pool_gain).astype(jnp.bfloat16)


def dispatch_plan(expert_ids, route_weight, ep_size):
    local_experts = EXPERTS // ep_size
    share = TOP if local_experts % GROUP_EXP == 0 else 1
    capacity = local_experts * CAP // share
    owners = expert_ids // local_experts
    ep_index = lax.iota(jnp.int32, ep_size)
    member = jnp.any(owners[:, :, None] == ep_index[None, None, :], axis=1)
    counts = member.astype(jnp.int32)
    rank = jnp.cumsum(counts, axis=0) - counts
    slot = jnp.where(member, rank, -1).T
    placing = slot[:, None, :] == lax.iota(jnp.int32, capacity)[None, :, None]
    dense_weight = jnp.sum(
        jnp.where(
            expert_ids[:, :, None] == lax.iota(jnp.int32, EXPERTS)[None, None, :],
            route_weight[:, :, None],
            0.0,
        ),
        axis=1,
    )
    dense_weight = dense_weight.reshape(-1, ep_size, local_experts)
    slot_weight = jnp.einsum(
        "ecn,nej->ecj", placing.astype(jnp.float32), dense_weight, precision=lax.Precision.HIGHEST
    )
    return (placing.astype(jnp.bfloat16).reshape(ep_size * capacity, -1), slot_weight, capacity)


def body(
    pool_input,
    pool_gain,
    mix_weight,
    moe_input,
    moe_gain,
    expert_ids,
    route_weight,
    gate_weight,
    up_weight,
    down_weight,
):
    pooled = pool_mixer(pool_input, pool_gain)
    regrouped = lax.all_to_all(pooled, "tp", split_axis=0, concat_axis=1, tiled=True)
    mixed_sum = jnp.dot(
        regrouped,
        lax.all_gather(mix_weight, "tp", axis=0, tiled=True),
        preferred_element_type=jnp.float32,
    )
    mixed_out = mixed_sum.astype(jnp.bfloat16)
    inputs = moe_input.astype(jnp.float32)
    scale_rows = lax.rsqrt(jnp.mean(inputs * inputs, axis=-1, keepdims=True) + eps_norm)
    normed = (inputs * scale_rows * moe_gain).astype(jnp.bfloat16)
    ep_size = lax.axis_size("ep")
    placing, slot_weight, capacity = dispatch_plan(expert_ids, route_weight, ep_size)
    outgoing = jnp.dot(placing, normed, preferred_element_type=jnp.float32).astype(jnp.bfloat16)
    arrived = lax.all_to_all(outgoing, "ep", split_axis=0, concat_axis=0, tiled=True)
    weights = lax.all_to_all(slot_weight, "ep", split_axis=0, concat_axis=0, tiled=True)
    weights = weights.reshape(ep_size * capacity, -1)
    tokens = lax.all_gather(arrived, "tp", axis=0, tiled=True)
    weights = lax.all_gather(weights, "tp", axis=0, tiled=True)
    gate_part = jnp.einsum("nd,edf->enf", tokens, gate_weight, preferred_element_type=jnp.float32)
    upward = jnp.einsum("nd,edf->enf", tokens, up_weight, preferred_element_type=jnp.float32)
    hidden = (jax.nn.silu(gate_part) * upward * weights.T[:, :, None]).astype(jnp.bfloat16)
    partial = jnp.einsum("enf,edf->nd", hidden, down_weight, preferred_element_type=jnp.float32)
    reduced = lax.psum_scatter(partial.astype(jnp.bfloat16), "tp", scatter_dimension=0, tiled=True)
    returned = lax.all_to_all(reduced, "ep", split_axis=0, concat_axis=0, tiled=True)
    combined = lax.dot_general(
        placing, returned, (((0,), (0,)), ((), ())), preferred_element_type=jnp.float32
    )
    moe_out = combined.astype(jnp.bfloat16)
    return (mixed_out, moe_out)


def solution(mesh):
    return jax.shard_map(
        body,
        mesh=mesh,
        in_specs=(
            P("ep", "tp"),
            P("tp"),
            P("tp", None),
            P(("ep", "tp"), None),
            P(),
            P(("ep", "tp"), None),
            P(("ep", "tp"), None),
            P("ep", None, "tp"),
            P("ep", None, "tp"),
            P("ep", None, "tp"),
        ),
        out_specs=(P(("ep", "tp"), None), P(("ep", "tp"), None)),
        check_vma=False,
    )
```

profile of v0, /device:TPU:0, one launch (start us, length us, event | category | flops | bytes accessed | tf_op | source)
XLA Modules:
  0.0 379.1 jit_solution(9585453362862034271)
XLA Ops:
  7.2 0.0 copy-start
  7.2 0.0 all-gather.5.cloned.1.call-start
  7.2 0.8 and_select_fusion
  8.1 1.2 reduce-window.6
  9.3 0.1 slice.68
  9.4 0.1 copy.31
  9.5 0.1 copy.32
  9.6 0.1 add_bitcast_fusion
  9.7 0.1 eq.111
  9.8 1.5 fusion.16
  11.3 0.1 bitcast_compare_fusion
  11.5 0.0 copy-start.2
  11.5 0.0 copy-start.3
  11.5 1.9 convolution_convert_fusion
  13.4 24.9 %all_to_all.45 = bf16[4,96,2048]{2,1,0:T(8,128)(2,1)} all-to-all(bf16[4,96,2048]{2,1,0:T(8,128)(2,1)S(1)} %bitcast.72), channel_id=1, replica_groups=mesh['ep'=4,'tp'=8] {'ep'}, dimensions={0} | all-to-all | bytes 3145728 | tf_op jit(solution)/shard_map/all_to_all | solution.py:102
  38.3 0.0 all-gather.5.cloned.1.call-update
  38.3 0.0 reduce-scatter.2.cloned.1.call-start
  38.4 0.0 copy-done.2
  38.4 0.0 copy-done.3
  38.4 0.3 fusion.28
  38.7 7.0 %all_to_all.46 = f32[4,96,4]{1,2,0:T(4,128)S(1)} all-to-all(f32[4,96,4]{1,2,0:T(4,128)S(1)} %fusion.28), channel_id=1, replica_groups=mesh['ep'=4,'tp'=8] {'ep'}, dimensions={0} | all-to-all | bytes 12288 | tf_op jit(solution)/shard_map/all_to_all | solution.py:103
  45.7 0.1 reshape.89
  45.8 17.4 %all_gather.11 = f32[3072,4]{0,1:T(4,128)S(1)} all-gather(f32[384,4]{0,1:T(4,128)S(1)} %reshape.89), channel_id=1, replica_groups=mesh['ep'=4,'tp'=8] {'tp'}, dimensions={0}, use_global_device_ids=true | all-gather | bytes 55296 | tf_op jit(solution)/shard_map/all_gather | solution.py:106
  63.2 92.0 %all-gather.5.cloned.1.call-done = bf16[3072,2048]{1,0:T(8,128)(2,1)} async-done(((bf16[384,2048]{1,0:T(8,128)(2,1)}), bf16[3072,2048]{1,0:T(8,128)(2,1)}) %all-gather.5.cloned.1.call-update) | async-done | bytes 12582928 | tf_op jit(solution)/shard_map/all_gather | solution.py:105
  155.2 12.0 %fusion.2 = f32[3072,4,128]{2,0,1:T(8,128)} fusion(bf16[4,2048,128]{2,1,0:T(8,128)(2,1)} %param.17, bf16[3072,2048]{1,0:T(8,128)(2,1)} %all-gather.5.cloned.1.call-done), kind=kOutput, calls=%fused_computation.3 | convolution fusion | flops 6442450944 | bytes 20971520 | tf_op jit(solution)/shard_map/nd,edf->enf/dot_general | solution.py:107
  167.2 0.0 copy-done
  167.2 19.4 %bitcast_convert_fusion = bf16[3072,2048]{1,0:T(8,128)(2,1)} fusion(bf16[4,2048,128]{2,1,0:T(8,128)(2,1)S(1)} %copy-done, f32[3072,4,128]{2,0,1:T(8,128)} %fusion.2, bf16[4,2048,128]{2,1,0:T(8,128)(2,1)} %param.18, bf16[3072,2048]{1,0:T(8,128)(2,1)} %all-gather.5.cloned.1.call-done, f32[4,3072]{1,0:T(4,128)S(1)} %bitcast.77), kind=kOutput, calls=%fused_computation | convolution fusion | flops 12902203392 | bytes 35700736 | tf_op jit(solution)/shard_map/enf,edf->nd/dot_general | solution.py:110
  186.6 0.0 reduce-scatter.2.cloned.1.call-update
  186.6 0.0 copy-start.4
  186.6 0.0 all-gather.3.cloned.1.call-start
  186.7 0.7 all-gather.3.cloned.1.call-update
  187.4 0.2 copy-done.1
  187.6 3.3 collective-permute-start
  190.9 1.2 collective-permute-done
  192.2 0.1 maximum_convert_fusion
  192.2 0.1 slice_add_fusion.1
  192.3 0.1 slice_add_fusion
  192.4 0.1 slice_add_fusion.2
  192.4 0.0 copy-done.4
  192.4 0.4 fusion.23
  192.8 16.7 %all_to_all.47 = bf16[8,128,128]{2,1,0:T(8,128)(2,1)S(1)} all-to-all(bf16[8,128,128]{2,1,0:T(8,128)(2,1)S(1)} %bitcast.74), channel_id=1, replica_groups=mesh['ep'=4,'tp'=8] {'tp'}, dimensions={0} | all-to-all | bytes 524288 | tf_op jit(solution)/shard_map/all_to_all | solution.py:89
  209.5 108.7 %reduce-scatter.2.cloned.1.call-done = bf16[384,2048]{1,0:T(8,128)(2,1)} async-done(((bf16[3072,2048]{1,0:T(8,128)(2,1)}), bf16[384,2048]{1,0:T(8,128)(2,1)}) %reduce-scatter.2.cloned.1.call-update) | async-done | bytes 1572880 | tf_op jit(solution)/shard_map/reduce_scatter | solution.py:111
  318.2 4.3 %all-to-all-start.3 = ((bf16[4,96,2048]{2,1,0:T(8,128)(2,1)}), bf16[4,96,2048]{2,1,0:T(8,128)(2,1)}, u32[]{:S(2)}, u32[]{:S(2)}) async-start(bf16[4,96,2048]{2,1,0:T(8,128)(2,1)} %bitcast.73), calls=%async_computation.4 | async-start | bytes 3145728 | tf_op jit(solution)/shard_map/all_to_all | solution.py:112
  322.6 0.2 copy.30
  322.7 42.9 %all-gather.3.cloned.1.call-done = bf16[1024,2048]{1,0:T(8,128)(2,1)} async-done(((bf16[128,2048]{1,0:T(8,128)(2,1)}), bf16[1024,2048]{1,0:T(8,128)(2,1)}) %all-gather.3.cloned.1.call-update) | async-done | bytes 4194320 | tf_op jit(solution)/shard_map/all_gather | solution.py:92
  365.7 3.7 convolution_convert_fusion.1
  369.4 0.0 all-to-all-done.3
  369.4 3.1 fusion.15
  (17 shorter events, 0.2 us)
Async XLA Ops:
  7.2 160.0 %copy-start = (bf16[4,2048,128]{2,1,0:T(8,128)(2,1)S(1)}, bf16[4,2048,128]{2,1,0:T(8,128)(2,1)}, u32[]{:S(2)}) copy-start(bf16[4,2048,128]{2,1,0:T(8,128)(2,1)} %param.19) | copy-start | bytes 6291460
  7.2 148.0 %all-gather.5.cloned.1.call-start = ((), (), s32[]{:S(2)}) async-start(), calls=%async_computation.6 | async-start | bytes 14155776 | tf_op jit(solution)/shard_map/all_gather | solution.py:105
  11.5 26.9 %copy-start.2 = (s32[256,2]{0,1:T(2,128)S(1)}, s32[256,2]{0,1:T(2,128)}, u32[]{:S(2)}) copy-start(s32[256,2]{0,1:T(2,128)} %param.15) | copy-start | bytes 6148
  11.5 26.9 %copy-start.3 = (f32[256,2]{0,1:T(2,128)S(1)}, f32[256,2]{0,1:T(2,128)}, u32[]{:S(2)}) copy-start(f32[256,2]{0,1:T(2,128)} %param.16) | copy-start | bytes 6148
  38.3 279.9 %reduce-scatter.2.cloned.1.call-start = ((), (), s32[]{:S(2)}) async-start(), calls=%async_computation.7 | async-start | bytes 14155776 | tf_op jit(solution)/shard_map/reduce_scatter | solution.py:111
  186.6 0.9 copy-start.1
  186.6 5.8 %copy-start.4 = (f32[128]{0:T(128)S(1)}, f32[128]{0:T(128)}, u32[]{:S(2)}) copy-start(f32[128]{0:T(128)} %param.11) | copy-start | bytes 1540
  186.6 179.0 %all-gather.3.cloned.1.call-start = ((), (), s32[]{:S(2)}) async-start(), calls=%async_computation.5 | async-start | bytes 4718592 | tf_op jit(solution)/shard_map/all_gather | solution.py:92
  187.6 4.6 %collective-permute-start = (bf16[15,128]{1,0:T(8,128)(2,1)S(1)}, bf16[15,128]{1,0:T(8,128)(2,1)S(1)}, u32[]{:S(2)}, u32[]{:S(2)}) collective-permute-start(bf16[15,128]{1,0:T(8,128)(2,1)S(1)} %slice.43), channel_id=1, source_target_pairs={{0,8},{8,16},{16,24},{1,9},{9,17},{17,25},{2,10},{10,18},{18,26},{... | collective-permute-start | bytes 11528 | tf_op jit(solution)/shard_map/ppermute | solution.py:17
  318.2 51.2 %all-to-all-start.3 = ((bf16[4,96,2048]{2,1,0:T(8,128)(2,1)}), bf16[4,96,2048]{2,1,0:T(8,128)(2,1)}, u32[]{:S(2)}, u32[]{:S(2)}) async-start(bf16[4,96,2048]{2,1,0:T(8,128)(2,1)} %bitcast.73), calls=%async_computation.4 | async-start | bytes 3145728 | tf_op jit(solution)/shard_map/all_to_all | solution.py:112
Sparse Core Ops, SparseCore 0:
  38.4 116.7 all-gather.4
  186.7 131.4 reduce-scatter.1
  319.8 45.8 all-gather.2
where the time goes:
time: 380 us; the launch traced here: 379 us
  waiting for transfers between devices  246 us (65%)
  blocking collectives  65.9 us (17%)
  matrix products  40.5 us (11%)
  between operations  13.9 us (4%)
  starting transfers between devices  7.76 us (2%)
  other arithmetic  4.48 us (1%)
    reduce_scatter x1, waiting for transfers between devices, body(): lax.psum_scatter(partial.astype(jnp.bfloat16), 'tp', scatter_dimension=0,...  109 us
    all_gather x1, waiting for transfers between devices, body(): tokens = lax.all_gather(arrived, 'tp', axis=0, tiled=True)  92 us
    all_gather x1, waiting for transfers between devices, body(): lax.all_gather(mix_weight, 'tp', axis=0, tiled=True)  42.9 us
    all_to_all x1, blocking collectives, body(): lax.all_to_all(outgoing, 'ep', split_axis=0, concat_axis=0, tiled=True)  24.9 us
    dot_general x1, matrix products, body(): jnp.einsum('enf,edf->nd', hidden, down_weight, preferred_element_type=jnp...  19.4 us
    all_gather x1, blocking collectives, body(): weights = lax.all_gather(weights, 'tp', axis=0, tiled=True)  17.4 us
    all_to_all x1, blocking collectives, body(): lax.all_to_all(pooled, 'tp', split_axis=0, concat_axis=1, tiled=True)  16.7 us
    dot_general x1, matrix products, body(): jnp.einsum('nd,edf->enf', tokens, gate_weight, preferred_element_type=jnp...  12 us
  transfers between devices with their start and end apart: 5, of which 4 were waited for; matrix products, arithmetic and copies ran while one was open for 1% of the time, Pallas kernels for 0%

commit v1 on v0

--- a/solution.py
+++ b/solution.py
@@ -2,6 +2,7 @@
 import jax.numpy as jnp
 from jax import lax
 from jax.sharding import PartitionSpec as P
+from jax.lax import all_gather
 
 GROUP_CH = 256
 EXPERTS = 16
@@ -102,8 +103,11 @@
     arrived = lax.all_to_all(outgoing, "ep", split_axis=0, concat_axis=0, tiled=True)
     weights = lax.all_to_all(slot_weight, "ep", split_axis=0, concat_axis=0, tiled=True)
     weights = weights.reshape(ep_size * capacity, -1)
-    tokens = lax.all_gather(arrived, "tp", axis=0, tiled=True)
-    weights = lax.all_gather(weights, "tp", axis=0, tiled=True)
+    tokens, weights = jnp.split(
+        all_gather(jnp.concatenate([arrived, weights], 1), "tp", axis=0, tiled=True),
+        [arrived.shape[1]],
+        1,
+    )
     gate_part = jnp.einsum("nd,edf->enf", tokens, gate_weight, preferred_element_type=jnp.float32)
     upward = jnp.einsum("nd,edf->enf", tokens, up_weight, preferred_element_type=jnp.float32)
     hidden = (jax.nn.silu(gate_part) * upward * weights.T[:, :, None]).astype(jnp.bfloat16)

time: 380 us -> 515 us (1.36)
  waiting for transfers between devices: 246 us -> 406 us
  blocking collectives: 65.9 us -> 16.7 us
  starting transfers between devices: 7.76 us -> 17.4 us
  matrix products: 40.5 us -> 46.2 us
    all_gather x1, waiting for transfers between devices: 92 us -> 233 us  [body(): all_gather(jnp.concatenate([arrived, weights], 1), 'tp', axis=0, tiled=True)]
    all_to_all x2 -> x0, blocking collectives: 31.9 us -> none  [the longest x1 24.9 us: body(): lax.all_to_all(outgoing, 'ep', split_axis=0, concat_axis=0, tiled=True)]
    all_to_all x0 -> x2, waiting for transfers between devices: none -> 19.1 us  [the longest x1 19.1 us: body(): lax.all_to_all(outgoing, 'ep', split_axis=0, concat_axis=0, tiled=True)]
    all_gather x1 -> x0, blocking collectives: 17.4 us -> none  [body(): weights = lax.all_gather(weights, 'tp', axis=0, tiled=True)]
    all_to_all x0 -> x2, starting transfers between devices: none -> 9.54 us  [the longest x1 5.19 us: body(): lax.all_to_all(slot_weight, 'ep', split_axis=0, concat_axis=0, tiled=True)]
  transfers between devices with their start and end apart: 5 -> 7, of which waited for: 4 -> 5; matrix products, arithmetic and copies ran while one was open for 1% -> 2% of each run, Pallas kernels for 0% -> 0%
where the time goes in v1:
time: 515 us; the launch traced here: 514 us
  waiting for transfers between devices  406 us (79%)
  matrix products  46.2 us (9%)
  starting transfers between devices  17.4 us (3%)
  blocking collectives  16.7 us (3%)
  between operations  13.9 us (3%)
  other arithmetic  9.02 us (2%)
  local copies, waits for them, and re-layouts  5.43 us (1%)
    all_gather x1, waiting for transfers between devices, body(): all_gather(jnp.concatenate([arrived, weights], 1), 'tp', axis=0, tiled=True)  233 us
    reduce_scatter x1, waiting for transfers between devices, body(): lax.psum_scatter(partial.astype(jnp.bfloat16), 'tp', scatter_dimension=0,...  109 us
    all_gather x1, waiting for transfers between devices, body(): lax.all_gather(mix_weight, 'tp', axis=0, tiled=True)  42.9 us
    dot_general x1, matrix products, body(): jnp.einsum('enf,edf->nd', hidden, down_weight, preferred_element_type=jnp...  21.3 us
    all_to_all x1, waiting for transfers between devices, body(): lax.all_to_all(outgoing, 'ep', split_axis=0, concat_axis=0, tiled=True)  19.1 us
    all_to_all x1, blocking collectives, body(): lax.all_to_all(pooled, 'tp', split_axis=0, concat_axis=1, tiled=True)  16.7 us
    dot_general x1, matrix products, body(): jnp.einsum('nd,edf->enf', tokens, gate_weight, preferred_element_type=jnp...  13.9 us
  transfers between devices with their start and end apart: 7, of which 5 were waited for; matrix products, arithmetic and copies ran while one was open for 2% of the time, Pallas kernels for 0%

profile of v1, /device:TPU:0, one launch (start us, length us, event | category | flops | bytes accessed | tf_op | source)
XLA Modules:
  0.0 514.5 jit_solution(16789781629966021948)
XLA Ops:
  7.2 0.0 copy-start
  7.2 0.8 and_select_fusion
  8.1 1.2 reduce-window.6
  9.3 0.1 slice.68
  9.4 0.1 copy.36
  9.5 0.1 copy.37
  9.6 0.1 add_bitcast_fusion
  9.7 0.7 select_reduce_fusion
  10.4 0.9 fusion.22
  11.3 5.2 %all-to-all-start.2 = ((f32[4,96,4]{1,2,0:T(4,128)}), f32[4,96,4]{1,2,0:T(4,128)S(1)}, u32[]{:S(2)}, u32[]{:S(2)}) async-start(f32[4,96,4]{1,2,0:T(4,128)} %fusion.22), calls=%async_computation.2 | async-start | bytes 16384 | tf_op jit(solution)/shard_map/all_to_all | solution.py:104
  16.5 0.1 eq.111
  16.6 0.1 bitcast_compare_fusion
  16.7 1.5 fusion.10
  18.2 3.1 convolution_convert_fusion
  21.3 0.0 all-to-all-done.2
  21.3 4.3 all-to-all-start.1
  25.7 0.0 all-gather.5.cloned.1.call-start
  25.7 0.1 copy.41
  25.9 19.1 %all-to-all-done.1 = bf16[4,96,2048]{2,1,0:T(8,128)(2,1)} async-done(((bf16[4,96,2048]{2,1,0:T(8,128)(2,1)}), bf16[4,96,2048]{2,1,0:T(8,128)(2,1)}, u32[]{:S(2)}, u32[]{:S(2)}) %all-to-all-start.1) | async-done | bytes 1572896 | tf_op jit(solution)/shard_map/all_to_all | solution.py:103
  45.0 1.8 bitcast_convert_fusion.1
  46.8 2.1 pad_maximum_fusion
  48.8 0.0 all-gather.5.cloned.1.call-update
  48.9 0.0 reduce-scatter.2.cloned.1.call-start
  48.9 233.1 %all-gather.5.cloned.1.call-done = f32[3072,2052]{1,0:T(8,128)} async-done(((f32[384,2052]{1,0:T(8,128)}), f32[3072,2052]{1,0:T(8,128)}) %all-gather.5.cloned.1.call-update) | async-done | bytes 25214992 | tf_op jit(solution)/shard_map/all_gather | solution.py:107
  282.0 2.6 slice_bitcast_fusion.7
  284.7 1.9 copy.40
  286.6 13.9 %fusion.1 = f32[3072,4,128]{2,0,1:T(8,128)} fusion(bf16[4,2048,128]{2,1,0:T(8,128)(2,1)} %param.17, f32[3072,2052]{1,0:T(8,128)} %all-gather.5.cloned.1.call-done), kind=kOutput, calls=%fused_computation.3 | convolution fusion | flops 6442450944 | bytes 20971520 | tf_op jit(solution)/shard_map/nd,edf->enf/dot_general | solution.py:111
  300.4 21.3 %bitcast_convert_fusion = bf16[3072,2048]{1,0:T(8,128)(2,1)} fusion(bf16[4,2048,128]{2,1,0:T(8,128)(2,1)S(1)} %copy-done, f32[3072,4,128]{2,0,1:T(8,128)} %fusion.1, bf16[4,2048,128]{2,1,0:T(8,128)(2,1)} %param.18, f32[3072,2052]{1,0:T(8,128)} %all-gather.5.cloned.1.call-done, f32[4,3072]{1,0:T(4,128)S(1)} %copy.40), kind=kOutput, calls=%fused_computation.1 | convolution fusion | flops 12902203392 | bytes 35700736 | tf_op jit(solution)/shard_map/enf,edf->nd/dot_general | solution.py:114
  321.8 0.0 reduce-scatter.2.cloned.1.call-update
  321.8 0.0 copy-start.3
  321.8 0.0 all-gather.3.cloned.1.call-start
  321.9 0.7 all-gather.3.cloned.1.call-update
  322.5 0.2 copy-done.2
  322.7 3.4 collective-permute-start
  326.2 1.2 collective-permute-done
  327.4 0.1 maximum_convert_fusion
  327.5 0.1 slice_add_fusion.1
  327.5 0.1 slice_add_fusion
  327.6 0.1 slice_add_fusion.2
  327.7 0.4 fusion.17
  328.0 16.7 %all_to_all.42 = bf16[8,128,128]{2,1,0:T(8,128)(2,1)S(1)} all-to-all(bf16[8,128,128]{2,1,0:T(8,128)(2,1)S(1)} %bitcast.74), channel_id=1, replica_groups=mesh['ep'=4,'tp'=8] {'tp'}, dimensions={0} | all-to-all | bytes 524288 | tf_op jit(solution)/shard_map/all_to_all | solution.py:90
  344.7 108.8 %reduce-scatter.2.cloned.1.call-done = bf16[384,2048]{1,0:T(8,128)(2,1)} async-done(((bf16[3072,2048]{1,0:T(8,128)(2,1)}), bf16[384,2048]{1,0:T(8,128)(2,1)}) %reduce-scatter.2.cloned.1.call-update) | async-done | bytes 1572880 | tf_op jit(solution)/shard_map/reduce_scatter | solution.py:115
  453.5 4.4 all-to-all-start.3
  457.8 0.2 copy.35
  458.0 42.9 %all-gather.3.cloned.1.call-done = bf16[1024,2048]{1,0:T(8,128)(2,1)} async-done(((bf16[128,2048]{1,0:T(8,128)(2,1)}), bf16[1024,2048]{1,0:T(8,128)(2,1)}) %all-gather.3.cloned.1.call-update) | async-done | bytes 4194320 | tf_op jit(solution)/shard_map/all_gather | solution.py:93
  500.9 3.9 convolution_convert_fusion.1
  504.8 0.0 all-to-all-done.3
  504.8 3.1 fusion.9
  (19 shorter events, 0.2 us)
Async XLA Ops:
  7.2 293.3 %copy-start = (bf16[4,2048,128]{2,1,0:T(8,128)(2,1)S(1)}, bf16[4,2048,128]{2,1,0:T(8,128)(2,1)}, u32[]{:S(2)}) copy-start(bf16[4,2048,128]{2,1,0:T(8,128)(2,1)} %param.19) | copy-start | bytes 6291460
  11.3 10.0 %all-to-all-start.2 = ((f32[4,96,4]{1,2,0:T(4,128)}), f32[4,96,4]{1,2,0:T(4,128)S(1)}, u32[]{:S(2)}, u32[]{:S(2)}) async-start(f32[4,96,4]{1,2,0:T(4,128)} %fusion.22), calls=%async_computation.2 | async-start | bytes 16384 | tf_op jit(solution)/shard_map/all_to_all | solution.py:104
  21.3 23.7 %all-to-all-start.1 = ((bf16[4,96,2048]{2,1,0:T(8,128)(2,1)}), bf16[4,96,2048]{2,1,0:T(8,128)(2,1)}, u32[]{:S(2)}, u32[]{:S(2)}) async-start(bf16[4,96,2048]{2,1,0:T(8,128)(2,1)} %bitcast.72), calls=%async_computation.1 | async-start | bytes 3145728 | tf_op jit(solution)/shard_map/all_to_all | solution.py:103
  25.7 256.4 %all-gather.5.cloned.1.call-start = ((), (), s32[]{:S(2)}) async-start(), calls=%async_computation.6 | async-start | bytes 30081024 | tf_op jit(solution)/shard_map/all_gather | solution.py:107
  48.9 404.6 %reduce-scatter.2.cloned.1.call-start = ((), (), s32[]{:S(2)}) async-start(), calls=%async_computation.7 | async-start | bytes 14155776 | tf_op jit(solution)/shard_map/reduce_scatter | solution.py:115
  321.8 0.9 copy-start.2
  321.8 5.9 %copy-start.3 = (f32[128]{0:T(128)S(1)}, f32[128]{0:T(128)}, u32[]{:S(2)}) copy-start(f32[128]{0:T(128)} %param.11) | copy-start | bytes 1540
  321.8 179.1 %all-gather.3.cloned.1.call-start = ((), (), s32[]{:S(2)}) async-start(), calls=%async_computation.5 | async-start | bytes 4718592 | tf_op jit(solution)/shard_map/all_gather | solution.py:93
  322.7 4.7 collective-permute-start
  453.5 51.3 %all-to-all-start.3 = ((bf16[4,96,2048]{2,1,0:T(8,128)(2,1)}), bf16[4,96,2048]{2,1,0:T(8,128)(2,1)}, u32[]{:S(2)}, u32[]{:S(2)}) async-start(bf16[4,96,2048]{2,1,0:T(8,128)(2,1)} %bitcast.73), calls=%async_computation.4 | async-start | bytes 3145728 | tf_op jit(solution)/shard_map/all_to_all | solution.py:116
  500.9 7.0 %copy-start.1 = (bf16[4,2048,128]{2,1,0:T(8,128)(2,1)S(1)}, bf16[4,2048,128]{2,1,0:T(8,128)(2,1)}, u32[]{:S(2)}) copy-start(bf16[4,2048,128]{2,1,0:T(8,128)(2,1)} %param.19) | copy-start | bytes 6291460
Sparse Core Ops, SparseCore 0:
  49.0 232.9 all-gather.4
  321.9 131.5 reduce-scatter.1
  455.1 45.7 all-gather.2
